TPU v7x, 128 devices: a whole 4x4x4 slice. The times are simulated.
128 devices in a mesh: fs: 16 (over z, y), tp: 8 (over x, core).
Axes of the slice: x: 4, y: 4, z: 4, core: 2. Of those that a mesh axis runs over, the one named last changes fastest.
Arguments:
- tokens: bfloat16 [8192, 4096], P('fs'), may hold values from -6 to 6
- norm_gain: float32 [4096], P('fs'), may hold values from 0.1 to 1.9
- gate_train: float32 [16, 4096, 1024], P(None, 'fs', 'tp'), may hold values from -0.09375 to 0.09375
- up_train: float32 [16, 4096, 1024], P(None, 'fs', 'tp'), may hold values from -0.09375 to 0.09375
- down_train: float32 [16, 1024, 4096], P(None, 'fs', 'tp'), may hold values from -0.1875 to 0.1875
- shared_gate_train: float32 [4096, 1024], P('fs', 'tp'), may hold values from -0.09375 to 0.09375
- shared_up_train: float32 [4096, 1024], P('fs', 'tp'), may hold values from -0.09375 to 0.09375
- shared_down_train: float32 [1024, 4096], P('fs', 'tp'), may hold values from -0.1875 to 0.1875
- route_expert: int32 [8192, 2], P('fs'), may hold values from 0 to 15, all different within a row; in each aligned block of 512 rows (0 to 511, 512 to 1023, ...) at most 96 rows name the same one
- route_weight: float32 [8192, 2], P('fs'), may hold values from 0.1 to 1
Outputs:
- expert_gate: bfloat16 [16, 4096, 1024], P('fs', None, 'tp')
- expert_up: bfloat16 [16, 4096, 1024], P('fs', None, 'tp')
- expert_down: bfloat16 [16, 1024, 4096], P('fs', 'tp')
- shared_gate: bfloat16 [4096, 1024], P(None, 'tp')
- shared_up: bfloat16 [4096, 1024], P(None, 'tp')
- shared_down: bfloat16 [1024, 4096], P('tp')
- mixed: bfloat16 [8192, 4096], P('fs', 'tp')
Inputs may be any that keep to these rules, and one draw needn't show every extreme that they name: `route_expert`: each row names 2 different experts. Within each aligned block of 512 rows no expert is named by more than 96 rows, a bound that some block reaches in every draw.
All inputs are finite; a program needn't handle non-finite values.
Results may differ from a plain program's by a relative error of at most 0.015.
Values may be sent and summed in bfloat16 or wider, within the bound.
No kernel may reach another device: no remote copies, remote signals or barrier semaphores. Data moves between devices by JAX's collectives and lax.ppermute only.
A program may use at most 128 MiB of HBM per device.

v0:
```python
import jax
import jax.numpy as jnp
from jax import lax
from jax.sharding import PartitionSpec as P

norm_eps = 1e-06


def sent_together(arrays, axis, dim, along):
    widths = [a.shape[along] for a in arrays]
    both = jnp.concatenate(arrays, axis=along)
    result = lax.all_gather(both, axis, axis=dim, tiled=True)
    return tuple(jnp.split(result, [sum(widths[:k]) for k in range(1, len(widths))], axis=along))


def blockwise_down(hidden, weight_down, pieces):
    step_width = hidden.shape[1] // pieces
    total = jnp.zeros((hidden.shape[0], weight_down.shape[1]), jnp.float32)
    for block in range(pieces):
        term = jnp.dot(
            hidden[:, block * step_width : (block + 1) * step_width],
            weight_down[block * step_width : (block + 1) * step_width],
            preferred_element_type=jnp.float32,
        )
        total = total + term.astype(jnp.bfloat16).astype(jnp.float32)
    return total


def on_device(
    tokens,
    norm_gain,
    gate_train,
    up_train,
    down_train,
    shared_gate_train,
    shared_up_train,
    shared_down_train,
    route_expert,
    route_weight,
):
    gain_rows = norm_gain[None, :, None]
    gate_local = (gain_rows * gate_train).astype(jnp.bfloat16)
    up_local = (gain_rows * up_train).astype(jnp.bfloat16)
    expert_gate, expert_up = (
        lax.all_to_all(gate_local, "fs", split_axis=0, concat_axis=1, tiled=True),
        lax.all_to_all(up_local, "fs", split_axis=0, concat_axis=1, tiled=True),
    )
    expert_down = lax.all_to_all(
        lax.all_to_all(
            down_train.astype(jnp.bfloat16), "fs", split_axis=0, concat_axis=1, tiled=True
        ),
        "tp",
        split_axis=1,
        concat_axis=2,
        tiled=True,
    )
    shared_gate_local = (norm_gain[:, None] * shared_gate_train).astype(jnp.bfloat16)
    shared_up_local = (norm_gain[:, None] * shared_up_train).astype(jnp.bfloat16)
    shared_gate, shared_up, shared_down_rows = (
        *sent_together((shared_gate_local, shared_up_local), "fs", 0, 1),
        lax.all_gather(shared_down_train.astype(jnp.bfloat16), "fs", axis=0, tiled=True),
    )
    shared_down = lax.all_to_all(shared_down_rows, "tp", split_axis=0, concat_axis=1, tiled=True)
    tok_rows, model_width = tokens.shape
    top_count = route_expert.shape[1]
    experts = lax.axis_size("fs")
    pieces = lax.axis_size("tp")
    capacity = 3 * tok_rows * top_count // (2 * experts)
    columns = model_width // pieces
    values = tokens.astype(jnp.float32)
    normed = (
        values * lax.rsqrt(jnp.mean(values * values, axis=1, keepdims=True) + norm_eps)
    ).astype(jnp.bfloat16)
    pairs = route_expert.reshape(-1)
    chosen = (pairs[:, None] == jnp.arange(experts, dtype=jnp.int32)[None, :]).astype(jnp.int32)
    earlier = jnp.cumsum(chosen, axis=0) - chosen
    slot_of = jnp.sum(earlier * chosen, axis=1)
    target = pairs * capacity + slot_of
    matches = (target[:, None] == jnp.arange(experts * capacity, dtype=jnp.int32)[None, :]).astype(
        jnp.bfloat16
    )
    placing = jnp.sum(matches.reshape(tok_rows, top_count, experts * capacity), axis=1)
    own_columns = lax.dynamic_slice_in_dim(normed, lax.axis_index("tp") * columns, columns, 1)
    outgoing = jnp.einsum("ts,td->sd", placing, own_columns, preferred_element_type=jnp.float32)
    outgoing = outgoing.astype(jnp.bfloat16).reshape(experts, capacity, columns)
    arriving = lax.all_to_all(outgoing, "fs", split_axis=0, concat_axis=0, tiled=True)
    arrived = lax.all_gather(arriving, "tp", axis=2, tiled=True)
    arrived_rows = arrived.reshape(-1, model_width)
    gate_vals = jnp.dot(arrived_rows, expert_gate[0], preferred_element_type=jnp.float32)
    up_vals = jnp.dot(arrived_rows, expert_up[0], preferred_element_type=jnp.float32)
    expert_hidden = (jax.nn.silu(gate_vals) * up_vals).astype(jnp.bfloat16)
    shared_gate_vals = jnp.dot(normed, shared_gate, preferred_element_type=jnp.float32)
    shared_up_vals = jnp.dot(normed, shared_up, preferred_element_type=jnp.float32)
    shared_hidden = (jax.nn.silu(shared_gate_vals) * shared_up_vals).astype(jnp.bfloat16)
    down_by_columns = lax.all_to_all(expert_down[0], "tp", split_axis=1, concat_axis=0, tiled=True)
    hidden_whole, shared_whole = sent_together((expert_hidden, shared_hidden), "tp", 1, 0)
    expert_sums = blockwise_down(hidden_whole, down_by_columns, pieces)
    shared_sums = blockwise_down(shared_whole, shared_down_rows, pieces)
    returning = expert_sums.astype(jnp.bfloat16).reshape(experts, capacity, columns)
    returned = lax.all_to_all(returning, "fs", split_axis=0, concat_axis=0, tiled=True).reshape(
        experts * capacity, columns
    )
    picked = jnp.take(returned, target, axis=0).reshape(tok_rows, top_count, columns)
    routed = jnp.sum(route_weight[:, :, None] * picked.astype(jnp.float32), axis=1)
    mixed = (routed + shared_sums).astype(jnp.bfloat16)
    return (expert_gate, expert_up, expert_down, shared_gate, shared_up, shared_down, mixed)


def solution(mesh):
    placed = (
        P("fs", None),
        P("fs"),
        P(None, "fs", "tp"),
        P(None, "fs", "tp"),
        P(None, "fs", "tp"),
        P("fs", "tp"),
        P("fs", "tp"),
        P("fs", "tp"),
        P("fs", None),
        P("fs", None),
    )
    return jax.shard_map(
        on_device,
        mesh=mesh,
        in_specs=placed,
        out_specs=(
            P("fs", None, "tp"),
            P("fs", None, "tp"),
            P("fs", "tp", None),
            P(None, "tp"),
            P(None, "tp"),
            P("tp", None),
            P("fs", "tp"),
        ),
        check_vma=False,
    )
```

profile of v0, /device:TPU:0, one launch (start us, length us, event | category | flops | bytes accessed | tf_op | source)
XLA Modules:
  0.0 312.0 jit_solution(5884856145658552887)
XLA Ops:
  7.2 1.1 multiply_convert_fusion.3
  10.2 4.5 %reduce-window.6 = s32[16,8,128]{2,1,0:T(8,128)S(1)} reduce-window(s32[16,8,128]{2,1,0:T(8,128)S(1)} %fusion.51, s32[]{:T(128)} %constant.18.clone.1), window={size=1x1x128 pad=0_0x0_0x127_0}, to_apply=%region_0.0 | reduce-window | flops 2080768 | bytes 131076 | tf_op jit(solution)/shard_map/reduce-window
  17.0 3.1 fusion
  20.1 1.5 fusion.1
  21.6 1.0 convolution_convert_fusion
  23.6 33.0 %all_to_all.99 = bf16[16,96,512]{2,1,0:T(8,128)(2,1)} all-to-all(bf16[16,96,512]{2,1,0:T(8,128)(2,1)S(1)} %bitcast.97), channel_id=1, replica_groups=mesh['fs'=16,'tp'=8] {'fs'}, dimensions={0} | all-to-all | bytes 3145728 | tf_op jit(solution)/shard_map/all_to_all | solution.py:86
  56.6 3.5 %multiply_convert_fusion = (bf16[16,256,128]{2,1,0:T(8,128)(2,1)}, bf16[16,256,128]{2,1,0:T(8,128)(2,1)}) fusion(f32[16,256,128]{2,1,0:T(8,128)S(1)} %copy-done.11, f32[256]{0:T(256)S(1)} %copy-done.16, f32[16,256,128]{2,1,0:T(8,128)} %param.12), kind=kLoop, calls=%fused_computation.21 | loop fusion | flops 2097152 | bytes 6292480 | tf_op jit(solution)/shard_map/convert_element_type | solution.py:43
  60.1 3.7 %all-to-all-start = ((bf16[16,256,128]{2,1,0:T(8,128)(2,1)}), bf16[16,256,128]{2,1,0:T(8,128)(2,1)S(1)}, u32[]{:S(2)}, u32[]{:S(2)}) async-start(bf16[16,256,128]{2,1,0:T(8,128)(2,1)} %get-tuple-element.49), calls=%async_computation | async-start | bytes 2097152 | tf_op jit(solution)/shard_map/all_to_all | solution.py:45
  64.6 1.8 fusion.55
  66.4 1.0 copy-done.2
  67.4 1.2 fusion.57
  68.7 1.3 fusion.22
  70.0 8.6 %all-to-all-done = bf16[16,256,128]{2,1,0:T(8,128)(2,1)S(1)} async-done(((bf16[16,256,128]{2,1,0:T(8,128)(2,1)}), bf16[16,256,128]{2,1,0:T(8,128)(2,1)S(1)}, u32[]{:S(2)}, u32[]{:S(2)}) %all-to-all-start) | async-done | bytes 1048608 | tf_op jit(solution)/shard_map/all_to_all | solution.py:45
  78.6 3.7 %all-to-all-start.1 = ((bf16[16,256,128]{2,1,0:T(8,128)(2,1)}), bf16[16,256,128]{2,1,0:T(8,128)(2,1)S(1)}, u32[]{:S(2)}, u32[]{:S(2)}) async-start(bf16[16,256,128]{2,1,0:T(8,128)(2,1)} %get-tuple-element.48), calls=%async_computation.1 | async-start | bytes 2097152 | tf_op jit(solution)/shard_map/all_to_all | solution.py:46
  82.3 51.0 %all-gather.9.cloned.1.call-done = bf16[16,96,4096]{2,1,0:T(8,128)(2,1)} async-done(((bf16[16,96,512]{2,1,0:T(8,128)(2,1)}), bf16[16,96,4096]{2,1,0:T(8,128)(2,1)}) %all-gather.9.cloned.1.call-update) | async-done | bytes 12582928 | tf_op jit(solution)/shard_map/all_gather | solution.py:87
  133.2 6.4 %fusion.56 = f32[1536,128]{1,0:T(8,128)S(1)} fusion(bf16[1536,4096]{1,0:T(8,128)(2,1)} %bitcast.102, bf16[4096,128]{1,0:T(8,128)(2,1)S(1)} %bitcast.91), kind=kOutput, calls=%fused_computation.106 | convolution fusion | flops 1610612736 | bytes 14417920 | tf_op jit(solution)/shard_map/dot_general | solution.py:89
  139.7 7.0 %fusion.4 = bf16[1536,128]{1,0:T(8,128)(2,1)S(1)} fusion(bf16[1536,4096]{1,0:T(8,128)(2,1)} %bitcast.103, bf16[4096,128]{1,0:T(8,128)(2,1)S(1)} %bitcast.93, f32[1536,128]{1,0:T(8,128)S(1)} %fusion.56), kind=kOutput, calls=%fused_computation.19 | convolution fusion | flops 1611792384 | bytes 14811136 | tf_op jit(solution)/shard_map/dot_general | solution.py:90
  147.6 1.7 convert_element_type.153
  149.3 25.8 %all_to_all.100 = bf16[16,64,512]{2,1,0:T(8,128)(2,1)S(1)} all-to-all(bf16[16,64,512]{2,1,0:T(8,128)(2,1)S(1)} %convert_element_type.153), channel_id=1, replica_groups=mesh['fs'=16,'tp'=8] {'fs'}, dimensions={0} | all-to-all | bytes 2097152 | tf_op jit(solution)/shard_map/all_to_all | solution.py:49
  175.1 1.6 copy.87
  177.2 7.0 %reduce.1 = bf16[1024,512]{1,0:T(8,128)(2,1)S(1)} reduce(bf16[1024,1,512]{2,1,0:T(2,128)(2,1)S(1)} %bitcast.80, bf16[]{:T(256)} %broadcast.91), dimensions={1}, to_apply=%bitcast.77.reduce_sub_computation | reduce | bytes 2097154
  185.0 24.0 %all_to_all.101 = bf16[8,2,32768]{2,1,0:T(2,128)(2,1)S(1)} all-to-all(bf16[8,2,32768]{2,1,0:T(2,128)(2,1)S(1)} %reshape.154), channel_id=1, replica_groups=mesh['fs'=16,'tp'=8] {'tp'}, dimensions={0} | all-to-all | bytes 2097152 | tf_op jit(solution)/shard_map/all_to_all | solution.py:48
  209.1 4.2 %all-to-all-start.4 = ((bf16[8,128,512]{2,1,0:T(8,128)(2,1)}), bf16[8,128,512]{2,1,0:T(8,128)(2,1)}, u32[]{:S(2)}, u32[]{:S(2)}) async-start(bf16[8,128,512]{2,1,0:T(8,128)(2,1)} %bitcast.89), calls=%async_computation.4 | async-start | bytes 2097152 | tf_op jit(solution)/shard_map/all_to_all | solution.py:63
  213.3 1.1 reshape.155
  214.4 1.3 copy.83
  215.7 17.9 %all-to-all-done.4 = bf16[8,128,512]{2,1,0:T(8,128)(2,1)} async-done(((bf16[8,128,512]{2,1,0:T(8,128)(2,1)}), bf16[8,128,512]{2,1,0:T(8,128)(2,1)}, u32[]{:S(2)}, u32[]{:S(2)}) %all-to-all-start.4) | async-done | bytes 1048608 | tf_op jit(solution)/shard_map/all_to_all | solution.py:63
  233.6 3.8 %all-to-all-start.6 = ((bf16[128,8,512]{2,0,1:T(8,128)(2,1)}), bf16[128,8,512]{2,0,1:T(8,128)(2,1)S(1)}, u32[]{:S(2)}, u32[]{:S(2)}) async-start(bf16[128,8,512]{2,0,1:T(8,128)(2,1)} %bitcast.14), calls=%async_computation.6 | async-start | bytes 2097152 | tf_op jit(solution)/shard_map/all_to_all | solution.py:95
  238.1 1.6 copy.71
  239.7 1.3 copy.81
  241.0 1.6 copy.72
  242.6 1.3 copy.82
  244.0 9.3 %all-to-all-done.6 = bf16[128,8,512]{2,0,1:T(8,128)(2,1)S(1)} async-done(((bf16[128,8,512]{2,0,1:T(8,128)(2,1)}), bf16[128,8,512]{2,0,1:T(8,128)(2,1)S(1)}, u32[]{:S(2)}, u32[]{:S(2)}) %all-to-all-start.6) | async-done | bytes 1048608 | tf_op jit(solution)/shard_map/all_to_all | solution.py:95
  253.3 1.7 convolution_convert_fusion.7
  255.0 1.5 convolution_convert_fusion.6
  259.3 2.8 add_convert_fusion
  262.1 3.9 %all-to-all-start.7 = ((bf16[16,96,512]{2,1,0:T(8,128)(2,1)}), bf16[16,96,512]{2,1,0:T(8,128)(2,1)S(1)}, u32[]{:S(2)}, u32[]{:S(2)}) async-start(bf16[16,96,512]{2,1,0:T(8,128)(2,1)} %bitcast.24), calls=%async_computation.7 | async-start | bytes 3145728 | tf_op jit(solution)/shard_map/all_to_all | solution.py:100
  266.0 1.2 fusion.21
  267.2 1.2 fusion.20
  268.4 1.2 fusion.18
  269.6 1.2 fusion.16
  270.8 1.2 fusion.14
  272.0 1.2 fusion.12
  273.2 2.2 fusion.10
  275.4 15.1 %all-to-all-done.7 = bf16[16,96,512]{2,1,0:T(8,128)(2,1)S(1)} async-done(((bf16[16,96,512]{2,1,0:T(8,128)(2,1)}), bf16[16,96,512]{2,1,0:T(8,128)(2,1)S(1)}, u32[]{:S(2)}, u32[]{:S(2)}) %all-to-all-start.7) | async-done | bytes 1572896 | tf_op jit(solution)/shard_map/all_to_all | solution.py:100
  290.4 5.1 %gather_fusion = bf16[1024,512]{1,0:T(8,128)(2,1)} fusion(bf16[1536,512]{1,0:T(8,128)(2,1)S(1)} %bitcast.78, s32[1024]{0:T(1024)S(1)} %broadcast_clamp_fusion), kind=kCustom, calls=%fused_computation | custom fusion | bytes 2101248 | tf_op jit(solution)/shard_map/jit(_take)/gather | solution.py:103
  295.5 1.6 gather.7
  297.1 4.4 %multiply_reduce_fusion = f32[512,512]{1,0:T(8,128)S(1)} fusion(bf16[512,2,512]{2,1,0:T(2,128)(2,1)S(1)} %gather.7, pred[512,2]{1,0:T(8,128)(4,1)S(1)} %copy.79, f32[512,2]{1,0:T(8,128)S(1)} %copy.73), kind=kLoop, calls=%fused_computation.20 | loop fusion | flops 1835008 | bytes 2102272 | tf_op jit(solution)/shard_map/reduce_sum | solution.py:104
  301.5 2.0 fusion.8
  (80 shorter events, 13.5 us)
Async XLA Ops:
  7.2 57.4 %all-gather.5.cloned.1.call-start = ((), (), s32[]{:S(2)}) async-start(), calls=%async_computation.8 | async-start | bytes 2228224 | tf_op jit(solution)/shard_map/all_gather | solution.py:12
  9.0 124.2 %all-gather.9.cloned.1.call-start = ((), (), s32[]{:S(2)}) async-start(), calls=%async_computation.10 | async-start | bytes 14155776 | tf_op jit(solution)/shard_map/all_gather | solution.py:87
  15.5 4.6 %copy-start = (bf16[512,4096]{1,0:T(8,128)(2,1)S(1)}, bf16[512,4096]{1,0:T(8,128)(2,1)}, u32[]{:S(2)}) copy-start(bf16[512,4096]{1,0:T(8,128)(2,1)} %param.10) | copy-start | bytes 12582916
  21.6 1.9 copy-start.1
  23.6 33.0 %copy-start.11 = (f32[16,256,128]{2,1,0:T(8,128)S(1)}, f32[16,256,128]{2,1,0:T(8,128)}, u32[]{:S(2)}) copy-start(f32[16,256,128]{2,1,0:T(8,128)} %param.13) | copy-start | bytes 6291460
  23.6 33.0 %copy-start.16 = (f32[256]{0:T(256)S(1)}, f32[256]{0:T(256)}, u32[]{:S(2)}) copy-start(f32[256]{0:T(256)} %param.11) | copy-start | bytes 3076
  56.6 7.3 %copy-start.13 = (f32[64,512]{1,0:T(8,128)S(1)}, f32[64,512]{1,0:T(8,128)}, u32[]{:S(2)}) copy-start(f32[64,512]{1,0:T(8,128)} %param.17) | copy-start | bytes 393220
  60.1 18.4 %all-to-all-start = ((bf16[16,256,128]{2,1,0:T(8,128)(2,1)}), bf16[16,256,128]{2,1,0:T(8,128)(2,1)S(1)}, u32[]{:S(2)}, u32[]{:S(2)}) async-start(bf16[16,256,128]{2,1,0:T(8,128)(2,1)} %get-tuple-element.49), calls=%async_computation | async-start | bytes 2097152 | tf_op jit(solution)/shard_map/all_to_all | solution.py:45
  63.8 145.3 %all-gather.7.cloned.1.call-start = ((), (), s32[]{:S(2)}) async-start(), calls=%async_computation.9 | async-start | bytes 1114112 | tf_op jit(solution)/shard_map/all_gather | solution.py:61
  64.5 2.9 copy-start.2
  66.4 2.3 copy-start.10
  66.4 2.3 copy-start.12
  78.6 61.1 %copy-start.5 = (bf16[16,256,128]{2,1,0:T(8,128)(2,1)}, bf16[16,256,128]{2,1,0:T(8,128)(2,1)S(1)}, u32[]{:S(2)}) copy-start(bf16[16,256,128]{2,1,0:T(8,128)(2,1)S(1)} %all-to-all-done) | copy-start | bytes 3145732
  78.6 61.1 %all-to-all-start.1 = ((bf16[16,256,128]{2,1,0:T(8,128)(2,1)}), bf16[16,256,128]{2,1,0:T(8,128)(2,1)S(1)}, u32[]{:S(2)}, u32[]{:S(2)}) async-start(bf16[16,256,128]{2,1,0:T(8,128)(2,1)} %get-tuple-element.48), calls=%async_computation.1 | async-start | bytes 2097152 | tf_op jit(solution)/shard_map/all_to_all | solution.py:46
  82.2 171.0 %all-gather.11.cloned.1.call-start = ((), (), s32[]{:S(2)}) async-start(), calls=%async_computation.11 | async-start | bytes 4718592 | tf_op jit(solution)/shard_map/all_gather | solution.py:12
  139.7 7.0 %copy-start.7 = (bf16[16,256,128]{2,1,0:T(8,128)(2,1)}, bf16[16,256,128]{2,1,0:T(8,128)(2,1)S(1)}, u32[]{:S(2)}) copy-start(bf16[16,256,128]{2,1,0:T(8,128)(2,1)S(1)} %all-to-all-done.1) | copy-start | bytes 3145732
  209.1 24.5 %all-to-all-start.4 = ((bf16[8,128,512]{2,1,0:T(8,128)(2,1)}), bf16[8,128,512]{2,1,0:T(8,128)(2,1)}, u32[]{:S(2)}, u32[]{:S(2)}) async-start(bf16[8,128,512]{2,1,0:T(8,128)(2,1)} %bitcast.89), calls=%async_computation.4 | async-start | bytes 2097152 | tf_op jit(solution)/shard_map/all_to_all | solution.py:63
  214.4 22.9 %copy-start.14 = (s32[512,2]{0,1:T(2,128)S(1)}, s32[512,2]{0,1:T(2,128)}, u32[]{:S(2)}) copy-start(s32[512,2]{0,1:T(2,128)} %param.18) | copy-start | bytes 12292
  214.4 23.5 %copy-start.15 = (f32[512,2]{0,1:T(2,128)S(1)}, f32[512,2]{0,1:T(2,128)}, u32[]{:S(2)}) copy-start(f32[512,2]{0,1:T(2,128)} %param.19) | copy-start | bytes 12292
  233.6 19.7 %all-to-all-start.6 = ((bf16[128,8,512]{2,0,1:T(8,128)(2,1)}), bf16[128,8,512]{2,0,1:T(8,128)(2,1)S(1)}, u32[]{:S(2)}, u32[]{:S(2)}) async-start(bf16[128,8,512]{2,0,1:T(8,128)(2,1)} %bitcast.14), calls=%async_computation.6 | async-start | bytes 2097152 | tf_op jit(solution)/shard_map/all_to_all | solution.py:95
  253.3 3.3 %copy-start.3 = (bf16[2048,1024]{1,0:T(8,128)(2,1)S(1)}, bf16[2048,1024]{1,0:T(8,128)(2,1)}, u32[]{:S(2)}) copy-start(bf16[2048,1024]{1,0:T(8,128)(2,1)} %all-gather.11.cloned.1.call-done) | copy-start | bytes 12582916
  262.1 3.9 %copy-start.4 = (bf16[1024,512]{1,0:T(8,128)(2,1)S(1)}, bf16[1024,512]{1,0:T(8,128)(2,1)}, u32[]{:S(2)}) copy-start(bf16[1024,512]{1,0:T(8,128)(2,1)} %all-gather.7.cloned.1.call-done) | copy-start | bytes 3145732
  262.1 28.3 %all-to-all-start.7 = ((bf16[16,96,512]{2,1,0:T(8,128)(2,1)}), bf16[16,96,512]{2,1,0:T(8,128)(2,1)S(1)}, u32[]{:S(2)}, u32[]{:S(2)}) async-start(bf16[16,96,512]{2,1,0:T(8,128)(2,1)} %bitcast.24), calls=%async_computation.7 | async-start | bytes 3145728 | tf_op jit(solution)/shard_map/all_to_all | solution.py:100
  295.5 6.0 %copy-start.9 = (f32[512,512]{1,0:T(8,128)S(1)}, f32[512,512]{1,0:T(8,128)}, u32[]{:S(2)}) copy-start(f32[512,512]{1,0:T(8,128)} %fusion.10) | copy-start | bytes 3145732
  297.0 6.4 %copy-start.6 = (bf16[16,256,128]{2,1,0:T(8,128)(2,1)S(1)}, bf16[16,256,128]{2,1,0:T(8,128)(2,1)}, u32[]{:S(2)}) copy-start(bf16[16,256,128]{2,1,0:T(8,128)(2,1)} %copy-done.5) | copy-start | bytes 3145732
  297.1 7.4 %copy-start.8 = (bf16[16,256,128]{2,1,0:T(8,128)(2,1)S(1)}, bf16[16,256,128]{2,1,0:T(8,128)(2,1)}, u32[]{:S(2)}) copy-start(bf16[16,256,128]{2,1,0:T(8,128)(2,1)} %copy-done.7) | copy-start | bytes 3145732
Sparse Core Ops, SparseCore 0:
  10.7 52.8 all-gather.4
  65.3 67.9 all-gather.8
  135.9 44.8 all-gather.6
  183.0 52.5 all-gather.10
where the time goes:
time: 313 us; the launch traced here: 312 us
  waiting for transfers between devices  102 us (33%)
  blocking collectives  82.7 us (26%)
  matrix products  37 us (12%)
  other arithmetic  30.7 us (10%)
  local copies, waits for them, and re-layouts  25.9 us (8%)
  starting transfers between devices  19.4 us (6%)
  between operations  14.3 us (5%)
    all_gather x1, waiting for transfers between devices, on_device(): arrived = lax.all_gather(arriving, 'tp', axis=2, tiled=True)  51 us
    all_to_all x1, blocking collectives, on_device(): lax.all_to_all(outgoing, 'fs', split_axis=0, concat_axis=0, tiled=True)  33 us
    all_to_all x1, blocking collectives, on_device(): lax.all_to_all(down_train.astype(jnp.bfloat16), 'fs', split_axis=0, conca...  25.8 us
    all_to_all x1, blocking collectives, on_device(): lax.all_to_all(lax.all_to_all(down_train.astype(jnp.bfloat16), 'fs', spli...  24 us
    dot_general x16, matrix products, blockwise_down(): jnp.dot(hidden[:, block * step_width:(block + 1) * step_width], weight_do...  20.1 us
    all_to_all x1, waiting for transfers between devices, on_device(): lax.all_to_all(shared_down_rows, 'tp', split_axis=0, concat_axis=1, tiled...  17.9 us
    all_to_all x1, waiting for transfers between devices, on_device(): lax.all_to_all(returning, 'fs', split_axis=0, concat_axis=0, tiled=True)  15.1 us
    unnamed x44, local copies, waits for them, and re-layouts  11.2 us
  transfers between devices with their start and end apart: 9, of which 5 were waited for; matrix products, arithmetic and copies ran while one was open for 21% of the time, Pallas kernels for 0%

commit v1 on v0

--- a/solution.py
+++ b/solution.py
@@ -84,7 +84,9 @@
     outgoing = jnp.einsum("ts,td->sd", placing, own_columns, preferred_element_type=jnp.float32)
     outgoing = outgoing.astype(jnp.bfloat16).reshape(experts, capacity, columns)
     arriving = lax.all_to_all(outgoing, "fs", split_axis=0, concat_axis=0, tiled=True)
-    arrived = lax.all_gather(arriving, "tp", axis=2, tiled=True)
+    arrived = jnp.concatenate(
+        lax.all_to_all(jnp.stack([arriving] * lax.axis_size("tp")), "tp", 0, 0), axis=2
+    )
     arrived_rows = arrived.reshape(-1, model_width)
     gate_vals = jnp.dot(arrived_rows, expert_gate[0], preferred_element_type=jnp.float32)
     up_vals = jnp.dot(arrived_rows, expert_up[0], preferred_element_type=jnp.float32)

time: 313 us -> 416 us (1.33)
  waiting for transfers between devices: 102 us -> 183 us
  local copies, waits for them, and re-layouts: 25.9 us -> 51.4 us
  blocking collectives: 82.7 us -> 68.4 us
  starting transfers between devices: 19.4 us -> 28.5 us
    all_to_all x0 -> x1, waiting for transfers between devices: none -> 134 us  [on_device(): lax.all_to_all(jnp.stack([arriving] * lax.axis_size('tp')), 'tp', 0, 0)]
    all_gather x1 -> x0, waiting for transfers between devices: 51 us -> none  [on_device(): arrived = lax.all_gather(arriving, 'tp', axis=2, tiled=True)]
    reshape x0 -> x1, local copies, waits for them, and re-layouts: none -> 12.1 us  [on_device(): jnp.concatenate(lax.all_to_all(jnp.stack([arriving] * lax.axis_size('tp')...]
    all_to_all x1, waiting for transfers between devices: 0.01 us -> 10.5 us  [on_device(): lax.all_to_all(up_local, 'fs', split_axis=0, concat_axis=1, tiled=True)]
    all_to_all x1, waiting for transfers between devices: 8.59 us -> 0.01 us  [on_device(): lax.all_to_all(gate_local, 'fs', split_axis=0, concat_axis=1, tiled=True)]
    unnamed x44 -> x45, local copies, waits for them, and re-layouts: 11.2 us -> 18.6 us
    all_to_all x1, blocking collectives: 25.8 us -> 19.3 us  [on_device(): lax.all_to_all(down_train.astype(jnp.bfloat16), 'fs', split_axis=0, conca...]
    another operation x2 -> x3, local copies, waits for them, and re-layouts: 0.08 us -> 6.15 us  [the longest x1 6.07 us: on_device(): jnp.stack([arriving] * lax.axis_size('tp'))]
  transfers between devices with their start and end apart: 9 -> 9, of which waited for: 5 -> 5; matrix products, arithmetic and copies ran while one was open for 21% -> 18% of each run, Pallas kernels for 0% -> 0%
where the time goes in v1:
time: 416 us; the launch traced here: 415 us
  waiting for transfers between devices  183 us (44%)
  blocking collectives  68.4 us (16%)
  local copies, waits for them, and re-layouts  51.4 us (12%)
  matrix products  38.4 us (9%)
  other arithmetic  31.5 us (8%)
  starting transfers between devices  28.5 us (7%)
  between operations  14.3 us (3%)
    all_to_all x1, waiting for transfers between devices, on_device(): lax.all_to_all(jnp.stack([arriving] * lax.axis_size('tp')), 'tp', 0, 0)  134 us
    all_to_all x1, blocking collectives, on_device(): lax.all_to_all(outgoing, 'fs', split_axis=0, concat_axis=0, tiled=True)  30.7 us
    dot_general x16, matrix products, blockwise_down(): jnp.dot(hidden[:, block * step_width:(block + 1) * step_width], weight_do...  20.5 us
    all_to_all x1, blocking collectives, on_device(): lax.all_to_all(down_train.astype(jnp.bfloat16), 'fs', split_axis=0, conca...  19.3 us
    unnamed x45, local copies, waits for them, and re-layouts  18.6 us
    all_to_all x1, blocking collectives, on_device(): lax.all_to_all(lax.all_to_all(down_train.astype(jnp.bfloat16), 'fs', spli...  18.4 us
    all_to_all x1, waiting for transfers between devices, on_device(): lax.all_to_all(returning, 'fs', split_axis=0, concat_axis=0, tiled=True)  15.2 us
    all_to_all x1, waiting for transfers between devices, on_device(): lax.all_to_all(shared_down_rows, 'tp', split_axis=0, concat_axis=1, tiled...  13.6 us
  transfers between devices with their start and end apart: 9, of which 5 were waited for; matrix products, arithmetic and copies ran while one was open for 18% of the time, Pallas kernels for 0%

profile of v1, /device:TPU:0, one launch (start us, length us, event | category | flops | bytes accessed | tf_op | source)
XLA Modules:
  0.0 415.2 jit_solution(6412491783498018611)
XLA Ops:
  8.4 4.5 %reduce-window.6 = s32[16,8,128]{2,1,0:T(8,128)S(1)} reduce-window(s32[16,8,128]{2,1,0:T(8,128)S(1)} %fusion.51, s32[]{:T(128)} %constant.18.clone.1), window={size=1x1x128 pad=0_0x0_0x127_0}, to_apply=%region_0.0 | reduce-window | flops 2080768 | bytes 131076 | tf_op jit(solution)/shard_map/reduce-window
  15.0 3.2 fusion
  18.4 3.4 fusion.1
  21.8 2.0 convolution_convert_fusion
  23.9 30.7 %all_to_all.104 = bf16[16,96,512]{2,1,0:T(8,128)(2,1)S(1)} all-to-all(bf16[16,96,512]{2,1,0:T(8,128)(2,1)S(1)} %bitcast.103), channel_id=1, replica_groups=mesh['fs'=16,'tp'=8] {'fs'}, dimensions={0} | all-to-all | bytes 3145728 | tf_op jit(solution)/shard_map/all_to_all | solution.py:86
  54.6 6.1 %stack.2 = bf16[8,16,96,512]{3,2,1,0:T(8,128)(2,1)} broadcast(bf16[16,96,512]{2,1,0:T(8,128)(2,1)S(1)} %all_to_all.104), dimensions={1,2,3} | broadcast | bytes 14155776 | tf_op jit(solution)/shard_map/stack | solution.py:88
  60.7 5.6 %all-to-all-start.6 = ((bf16[8,16,96,512]{3,2,1,0:T(8,128)(2,1)}), bf16[8,16,96,512]{3,2,1,0:T(8,128)(2,1)}, u32[]{:S(2)}, u32[]{:S(2)}) async-start(bf16[8,16,96,512]{3,2,1,0:T(8,128)(2,1)} %stack.2), calls=%async_computation.6 | async-start | bytes 25165824 | tf_op jit(solution)/shard_map/all_to_all | solution.py:88
  68.0 3.5 multiply_convert_fusion
  71.5 134.4 %all-to-all-done.6 = bf16[8,16,96,512]{3,2,1,0:T(8,128)(2,1)} async-done(((bf16[8,16,96,512]{3,2,1,0:T(8,128)(2,1)}), bf16[8,16,96,512]{3,2,1,0:T(8,128)(2,1)}, u32[]{:S(2)}, u32[]{:S(2)}) %all-to-all-start.6) | async-done | bytes 12582944 | tf_op jit(solution)/shard_map/all_to_all | solution.py:88
  205.9 3.8 all-to-all-start
  209.7 1.8 fusion.55
  212.6 1.2 fusion.57
  213.9 1.3 fusion.22
  215.1 12.1 %copy.83 = bf16[16,96,8,512]{3,2,1,0:T(8,128)(2,1)S(1)} copy(bf16[16,96,8,512]{3,1,0,2:T(8,128)(2,1)} %bitcast.11) | data formatting | bytes 25165824 | tf_op jit(solution)/shard_map/reshape | solution.py:87
  227.2 8.1 %copy.89 = bf16[192,8,8,512]{3,1,2,0:T(8,128)(2,1)} copy(bf16[192,8,8,512]{3,2,1,0:T(8,128)(2,1)S(1)} %bitcast.82) | data formatting | bytes 25165824
  235.3 7.0 %all-to-all-start.1 = ((bf16[16,256,128]{2,1,0:T(8,128)(2,1)}), bf16[16,256,128]{2,1,0:T(8,128)(2,1)S(1)}, u32[]{:S(2)}, u32[]{:S(2)}) async-start(bf16[16,256,128]{2,1,0:T(8,128)(2,1)} %get-tuple-element.48), calls=%async_computation.1 | async-start | bytes 2097152 | tf_op jit(solution)/shard_map/all_to_all | solution.py:46
  242.4 6.4 %fusion.56 = f32[1536,128]{1,0:T(8,128)S(1)} fusion(bf16[1536,4096]{1,0:T(8,128)(2,1)} %bitcast.83, bf16[4096,128]{1,0:T(8,128)(2,1)S(1)} %bitcast.97), kind=kOutput, calls=%fused_computation.106 | convolution fusion | flops 1610612736 | bytes 14417920 | tf_op jit(solution)/shard_map/dot_general | solution.py:91
  248.8 10.5 %all-to-all-done.1 = bf16[16,256,128]{2,1,0:T(8,128)(2,1)S(1)} async-done(((bf16[16,256,128]{2,1,0:T(8,128)(2,1)}), bf16[16,256,128]{2,1,0:T(8,128)(2,1)S(1)}, u32[]{:S(2)}, u32[]{:S(2)}) %all-to-all-start.1) | async-done | bytes 1048608 | tf_op jit(solution)/shard_map/all_to_all | solution.py:46
  259.3 7.0 %fusion.4 = bf16[1536,128]{1,0:T(8,128)(2,1)S(1)} fusion(bf16[1536,4096]{1,0:T(8,128)(2,1)} %bitcast.84, bf16[4096,128]{1,0:T(8,128)(2,1)S(1)} %bitcast.99, f32[1536,128]{1,0:T(8,128)S(1)} %fusion.56), kind=kOutput, calls=%fused_computation.19 | convolution fusion | flops 1611792384 | bytes 14811136 | tf_op jit(solution)/shard_map/dot_general | solution.py:92
  267.2 1.7 convert_element_type.153
  268.9 19.3 %all_to_all.105 = bf16[16,64,512]{2,1,0:T(8,128)(2,1)S(1)} all-to-all(bf16[16,64,512]{2,1,0:T(8,128)(2,1)S(1)} %convert_element_type.153), channel_id=1, replica_groups=mesh['fs'=16,'tp'=8] {'fs'}, dimensions={0} | all-to-all | bytes 2097152 | tf_op jit(solution)/shard_map/all_to_all | solution.py:49
  288.2 1.6 copy.92
  290.3 7.0 %reduce.1 = bf16[1024,512]{1,0:T(8,128)(2,1)S(1)} reduce(bf16[1024,1,512]{2,1,0:T(2,128)(2,1)S(1)} %bitcast.86, bf16[]{:T(256)} %broadcast.93), dimensions={1}, to_apply=%bitcast.80.reduce_sub_computation | reduce | bytes 2097154
  298.2 18.4 %all_to_all.106 = bf16[8,2,32768]{2,1,0:T(2,128)(2,1)S(1)} all-to-all(bf16[8,2,32768]{2,1,0:T(2,128)(2,1)S(1)} %reshape.156), channel_id=1, replica_groups=mesh['fs'=16,'tp'=8] {'tp'}, dimensions={0} | all-to-all | bytes 2097152 | tf_op jit(solution)/shard_map/all_to_all | solution.py:48
  316.6 4.2 %all-to-all-start.4 = ((bf16[8,128,512]{2,1,0:T(8,128)(2,1)}), bf16[8,128,512]{2,1,0:T(8,128)(2,1)}, u32[]{:S(2)}, u32[]{:S(2)}) async-start(bf16[8,128,512]{2,1,0:T(8,128)(2,1)} %bitcast.95), calls=%async_computation.4 | async-start | bytes 2097152 | tf_op jit(solution)/shard_map/all_to_all | solution.py:63
  321.9 1.3 copy.87
  323.2 13.6 %all-to-all-done.4 = bf16[8,128,512]{2,1,0:T(8,128)(2,1)} async-done(((bf16[8,128,512]{2,1,0:T(8,128)(2,1)}), bf16[8,128,512]{2,1,0:T(8,128)(2,1)}, u32[]{:S(2)}, u32[]{:S(2)}) %all-to-all-start.4) | async-done | bytes 1048608 | tf_op jit(solution)/shard_map/all_to_all | solution.py:63
  336.8 3.8 all-to-all-start.7
  341.3 1.6 copy.74
  343.0 1.3 copy.85
  344.3 1.6 copy.75
  345.9 1.3 copy.86
  347.2 9.0 %all-to-all-done.7 = bf16[128,8,512]{2,0,1:T(8,128)(2,1)S(1)} async-done(((bf16[128,8,512]{2,0,1:T(8,128)(2,1)}), bf16[128,8,512]{2,0,1:T(8,128)(2,1)S(1)}, u32[]{:S(2)}, u32[]{:S(2)}) %all-to-all-start.7) | async-done | bytes 1048608 | tf_op jit(solution)/shard_map/all_to_all | solution.py:97
  356.2 1.7 convolution_convert_fusion.7
  357.9 1.5 convolution_convert_fusion.6
  362.2 2.8 add_convert_fusion
  365.1 3.8 all-to-all-start.8
  368.9 1.2 fusion.21
  370.1 1.2 fusion.20
  372.5 1.2 fusion.16
  373.7 1.2 fusion.14
  374.9 1.2 fusion.12
  376.1 2.2 fusion.10
  378.2 15.2 %all-to-all-done.8 = bf16[16,96,512]{2,1,0:T(8,128)(2,1)S(1)} async-done(((bf16[16,96,512]{2,1,0:T(8,128)(2,1)}), bf16[16,96,512]{2,1,0:T(8,128)(2,1)S(1)}, u32[]{:S(2)}, u32[]{:S(2)}) %all-to-all-start.8) | async-done | bytes 1572896 | tf_op jit(solution)/shard_map/all_to_all | solution.py:102
  393.4 5.1 %gather_fusion = bf16[1024,512]{1,0:T(8,128)(2,1)} fusion(bf16[1536,512]{1,0:T(8,128)(2,1)S(1)} %bitcast.81, s32[1024]{0:T(1024)S(1)} %broadcast_clamp_fusion), kind=kCustom, calls=%fused_computation | custom fusion | bytes 2101248 | tf_op jit(solution)/shard_map/jit(_take)/gather | solution.py:105
  398.5 1.5 gather.7
  400.0 4.4 %multiply_reduce_fusion = f32[512,512]{1,0:T(8,128)S(1)} fusion(bf16[512,2,512]{2,1,0:T(2,128)(2,1)S(1)} %gather.7, pred[512,2]{1,0:T(8,128)(4,1)S(1)} %copy.82, f32[512,2]{1,0:T(8,128)S(1)} %copy.76), kind=kLoop, calls=%fused_computation.20 | loop fusion | flops 1835008 | bytes 2102272 | tf_op jit(solution)/shard_map/reduce_sum | solution.py:106
  404.4 2.4 fusion.8
  (82 shorter events, 15.9 us)
Async XLA Ops:
  15.0 3.5 copy-start
  60.7 5.7 %copy-start.11 = (f32[256,128]{1,0:T(8,128)S(1)}, f32[256,128]{1,0:T(8,128)}, u32[]{:S(2)}) copy-start(f32[256,128]{1,0:T(8,128)} %param.15) | copy-start | bytes 393220
  60.7 5.7 %copy-start.12 = (f32[256,128]{1,0:T(8,128)S(1)}, f32[256,128]{1,0:T(8,128)}, u32[]{:S(2)}) copy-start(f32[256,128]{1,0:T(8,128)} %param.16) | copy-start | bytes 393220
  60.7 5.7 %copy-start.16 = (f32[256]{0:T(256)S(1)}, f32[256]{0:T(256)}, u32[]{:S(2)}) copy-start(f32[256]{0:T(256)} %param.11) | copy-start | bytes 3076
  60.7 6.6 %copy-start.13 = (f32[64,512]{1,0:T(8,128)S(1)}, f32[64,512]{1,0:T(8,128)}, u32[]{:S(2)}) copy-start(f32[64,512]{1,0:T(8,128)} %param.17) | copy-start | bytes 393220
  60.7 7.3 %copy-start.9 = (f32[16,256,128]{2,1,0:T(8,128)S(1)}, f32[16,256,128]{2,1,0:T(8,128)}, u32[]{:S(2)}) copy-start(f32[16,256,128]{2,1,0:T(8,128)} %param.13) | copy-start | bytes 6291460
  60.7 145.2 %all-to-all-start.6 = ((bf16[8,16,96,512]{3,2,1,0:T(8,128)(2,1)}), bf16[8,16,96,512]{3,2,1,0:T(8,128)(2,1)}, u32[]{:S(2)}, u32[]{:S(2)}) async-start(bf16[8,16,96,512]{3,2,1,0:T(8,128)(2,1)} %stack.2), calls=%async_computation.6 | async-start | bytes 25165824 | tf_op jit(solution)/shard_map/all_to_all | solution.py:88
  66.3 143.4 %all-gather.4.cloned.1.call-start = ((), (), s32[]{:S(2)}) async-start(), calls=%async_computation.9 | async-start | bytes 2228224 | tf_op jit(solution)/shard_map/all_gather | solution.py:12
  67.2 249.4 %all-gather.6.cloned.1.call-start = ((), (), s32[]{:S(2)}) async-start(), calls=%async_computation.10 | async-start | bytes 1114112 | tf_op jit(solution)/shard_map/all_gather | solution.py:61
  205.9 29.5 %all-to-all-start = ((bf16[16,256,128]{2,1,0:T(8,128)(2,1)}), bf16[16,256,128]{2,1,0:T(8,128)(2,1)S(1)}, u32[]{:S(2)}, u32[]{:S(2)}) async-start(bf16[16,256,128]{2,1,0:T(8,128)(2,1)} %get-tuple-element.49), calls=%async_computation | async-start | bytes 2097152 | tf_op jit(solution)/shard_map/all_to_all | solution.py:45
  209.7 2.9 copy-start.1
  211.6 3.6 copy-start.8
  211.6 3.6 copy-start.10
  235.3 13.5 %copy-start.4 = (bf16[16,256,128]{2,1,0:T(8,128)(2,1)}, bf16[16,256,128]{2,1,0:T(8,128)(2,1)S(1)}, u32[]{:S(2)}) copy-start(bf16[16,256,128]{2,1,0:T(8,128)(2,1)S(1)} %all-to-all-done) | copy-start | bytes 3145732
  235.3 23.9 %all-to-all-start.1 = ((bf16[16,256,128]{2,1,0:T(8,128)(2,1)}), bf16[16,256,128]{2,1,0:T(8,128)(2,1)S(1)}, u32[]{:S(2)}, u32[]{:S(2)}) async-start(bf16[16,256,128]{2,1,0:T(8,128)(2,1)} %get-tuple-element.48), calls=%async_computation.1 | async-start | bytes 2097152 | tf_op jit(solution)/shard_map/all_to_all | solution.py:46
  242.3 113.9 %all-gather.8.cloned.1.call-start = ((), (), s32[]{:S(2)}) async-start(), calls=%async_computation.11 | async-start | bytes 4718592 | tf_op jit(solution)/shard_map/all_gather | solution.py:12
  259.3 7.0 %copy-start.6 = (bf16[16,256,128]{2,1,0:T(8,128)(2,1)}, bf16[16,256,128]{2,1,0:T(8,128)(2,1)S(1)}, u32[]{:S(2)}) copy-start(bf16[16,256,128]{2,1,0:T(8,128)(2,1)S(1)} %all-to-all-done.1) | copy-start | bytes 3145732
  316.6 20.2 %all-to-all-start.4 = ((bf16[8,128,512]{2,1,0:T(8,128)(2,1)}), bf16[8,128,512]{2,1,0:T(8,128)(2,1)}, u32[]{:S(2)}, u32[]{:S(2)}) async-start(bf16[8,128,512]{2,1,0:T(8,128)(2,1)} %bitcast.95), calls=%async_computation.4 | async-start | bytes 2097152 | tf_op jit(solution)/shard_map/all_to_all | solution.py:63
  321.9 18.7 %copy-start.14 = (s32[512,2]{0,1:T(2,128)S(1)}, s32[512,2]{0,1:T(2,128)}, u32[]{:S(2)}) copy-start(s32[512,2]{0,1:T(2,128)} %param.18) | copy-start | bytes 12292
  321.9 19.3 %copy-start.15 = (f32[512,2]{0,1:T(2,128)S(1)}, f32[512,2]{0,1:T(2,128)}, u32[]{:S(2)}) copy-start(f32[512,2]{0,1:T(2,128)} %param.19) | copy-start | bytes 12292
  336.8 19.4 %all-to-all-start.7 = ((bf16[128,8,512]{2,0,1:T(8,128)(2,1)}), bf16[128,8,512]{2,0,1:T(8,128)(2,1)S(1)}, u32[]{:S(2)}, u32[]{:S(2)}) async-start(bf16[128,8,512]{2,0,1:T(8,128)(2,1)} %bitcast.14), calls=%async_computation.7 | async-start | bytes 2097152 | tf_op jit(solution)/shard_map/all_to_all | solution.py:97
  356.2 3.3 copy-start.2
  365.1 3.9 copy-start.3
  365.1 28.3 %all-to-all-start.8 = ((bf16[16,96,512]{2,1,0:T(8,128)(2,1)}), bf16[16,96,512]{2,1,0:T(8,128)(2,1)S(1)}, u32[]{:S(2)}, u32[]{:S(2)}) async-start(bf16[16,96,512]{2,1,0:T(8,128)(2,1)} %bitcast.24), calls=%async_computation.8 | async-start | bytes 3145728 | tf_op jit(solution)/shard_map/all_to_all | solution.py:102
  399.9 6.8 %copy-start.5 = (bf16[16,256,128]{2,1,0:T(8,128)(2,1)S(1)}, bf16[16,256,128]{2,1,0:T(8,128)(2,1)}, u32[]{:S(2)}) copy-start(bf16[16,256,128]{2,1,0:T(8,128)(2,1)} %copy-done.4) | copy-start | bytes 3145732
  400.0 7.8 %copy-start.7 = (bf16[16,256,128]{2,1,0:T(8,128)(2,1)S(1)}, bf16[16,256,128]{2,1,0:T(8,128)(2,1)}, u32[]{:S(2)}) copy-start(bf16[16,256,128]{2,1,0:T(8,128)(2,1)} %copy-done.6) | copy-start | bytes 3145732
Sparse Core Ops, SparseCore 0:
  69.8 42.9 all-gather.3
  115.5 41.8 all-gather.5
  267.3 30.5 all-gather.7
